TPU v7x, 32 devices: a whole 2x2x4 slice. The times are simulated.
32 devices in a mesh: tp: 8 (over z, y), dp: 4 (over x, core).
Axes of the slice: x: 2, y: 2, z: 4, core: 2. Of those that a mesh axis runs over, the one named last changes fastest.
Arguments:
- stream: bfloat16 [32, 4096], P('dp', 'tp'), may hold values from -6 to 6
- query_weight: bfloat16 [2, 4096, 3072], P(None, 'dp', 'tp'), may hold values from -0.09375 to 0.09375
- key_weight: bfloat16 [2, 4096, 3072], P(None, 'dp', 'tp'), may hold values from -0.09375 to 0.09375
- value_weight: bfloat16 [2, 4096, 3072], P(None, 'dp', 'tp'), may hold values from -0.09375 to 0.09375
- outgate_weight: bfloat16 [2, 4096, 3072], P(None, 'dp', 'tp'), may hold values from -0.09375 to 0.09375
- gate_weight: bfloat16 [2, 4096, 32], replicated, may hold values from -0.09375 to 0.09375
- gate_bias: float32 [2, 32], replicated, may hold values from -1 to 3
- output_weight: bfloat16 [2, 3072, 4096], P(None, 'dp', 'tp'), may hold values from -0.109375 to 0.109375
- norm_gain: float32 [2, 4096], replicated, may hold values from 0.1 to 1.9
- matrix_state: float32 [2, 32, 192, 16, 192], P(None, 'dp', 'tp'), may hold values from -0.6 to 0.6
- normalizer_state: float32 [2, 32, 16, 192], P(None, 'dp'), may hold values from -0.6 to 0.6
- stabilizer_state: float32 [2, 32, 16], P(None, 'dp'), may hold values from -4 to 4
Outputs:
- out_stream: bfloat16 [32, 4096], P('dp', 'tp')
- new_matrix: float32 [2, 32, 192, 16, 192], P(None, 'dp', 'tp')
- new_normalizer: float32 [2, 32, 16, 192], P(None, 'dp')
- new_stabilizer: float32 [2, 32, 16], P(None, 'dp')
All inputs are finite; a program needn't handle non-finite values.
Results may differ from a plain program's by a relative error of at most 0.015.
Values may be sent and summed in bfloat16 or wider, within the bound.
A program may use at most 128 MiB of HBM per device.

v0:
```python
import jax
import jax.numpy as jnp
from jax import lax
from jax.sharding import PartitionSpec as P

residual_scale = 8.0**0.25
norm_eps = 1e-05


def normalize(values_in, gain):
    upcast = values_in.astype(jnp.float32)
    average = jnp.mean(upcast, axis=-1, keepdims=True)
    variance = jnp.mean(jnp.square(upcast - average), axis=-1, keepdims=True)
    return ((upcast - average) * lax.rsqrt(variance + norm_eps) * gain).astype(jnp.bfloat16)


def widen_rows(local_cols):
    return lax.all_gather(local_cols, "tp", axis=1, tiled=True)


def shards(
    stream,
    query_weight,
    key_weight,
    value_weight,
    outgate_weight,
    gate_weight,
    gate_bias,
    output_weight,
    norm_gain,
    matrix_state,
    normalizer_state,
    stabilizer_state,
):
    head_count = gate_bias.shape[1] // 2
    head_size = normalizer_state.shape[3]
    seq_local = stream.shape[0]
    feat_local = stream.shape[1]
    col_local = query_weight.shape[2]
    feat_offset = lax.axis_index("tp") * feat_local
    x_local = stream
    x_full = widen_rows(stream)
    new_mats, new_norms, new_stabs = ([], [], [])
    for block_no in range(gate_bias.shape[0]):
        weight_set = (
            query_weight[block_no],
            key_weight[block_no],
            value_weight[block_no],
            outgate_weight[block_no],
        )
        columns = x_full
        joined = jnp.concatenate(
            (
                lax.all_gather(weight_set[0], "dp", axis=0, tiled=True),
                lax.all_gather(weight_set[1], "dp", axis=0, tiled=True),
                lax.all_gather(weight_set[2], "dp", axis=0, tiled=True),
                lax.all_gather(weight_set[3], "dp", axis=0, tiled=True),
            ),
            axis=1,
        )
        packed = jnp.dot(columns, joined, preferred_element_type=jnp.float32)
        projected = packed.astype(jnp.bfloat16)
        query_part = projected[:, :col_local]
        key_part = projected[:, col_local : 2 * col_local]
        value_part = projected[:, 2 * col_local : 3 * col_local]
        outgate_part = projected[:, 3 * col_local :]
        query_full, key_full = (
            lax.all_gather(query_part, "tp", axis=1, tiled=True),
            lax.all_gather(key_part, "tp", axis=1, tiled=True),
        )
        gate_pre = (
            jnp.dot(x_full, gate_weight[block_no], preferred_element_type=jnp.float32)
            + gate_bias[block_no]
        )
        log_in = gate_pre[:, :head_count]
        log_forget = jax.nn.log_sigmoid(gate_pre[:, head_count:])
        old_stab = stabilizer_state[block_no]
        stab_new = jnp.maximum(log_forget + old_stab, log_in)
        retain = jnp.exp(log_forget + old_stab - stab_new)
        admit = jnp.exp(log_in - stab_new)
        queries = query_full.astype(jnp.float32).reshape(seq_local, head_count, head_size)
        keys = key_full.astype(jnp.float32).reshape(
            seq_local, head_count, head_size
        ) * head_size ** (-0.5)
        values = value_part.astype(jnp.float32).reshape(seq_local, -1, head_count)
        matrix = (
            retain[:, None, :, None] * matrix_state[block_no]
            + admit[:, None, :, None] * values[..., None] * keys[:, None, :, :]
        )
        norm_new = retain[..., None] * normalizer_state[block_no] + admit[..., None] * keys
        numerator = jnp.einsum("shd,sehd->seh", queries, matrix, precision=lax.Precision.HIGHEST)
        denominator = jnp.sum(queries * norm_new, axis=-1)
        divisor = jnp.maximum(jnp.abs(denominator), 1.0)
        readout = (numerator / divisor[:, None, :]).reshape(seq_local, col_local)
        hidden = (readout * jax.nn.sigmoid(outgate_part.astype(jnp.float32))).astype(jnp.bfloat16)
        hidden_full = lax.all_gather(hidden, "tp", axis=1, tiled=True)
        branch = jnp.dot(
            hidden_full,
            lax.all_gather(output_weight[block_no], "dp", axis=0, tiled=True),
            preferred_element_type=jnp.float32,
        )
        summed = (residual_scale * x_local.astype(jnp.float32) + branch).astype(jnp.bfloat16)
        x_full = normalize(widen_rows(summed), norm_gain[block_no])
        x_local = lax.dynamic_slice_in_dim(x_full, feat_offset, feat_local, 1)
        new_mats.append(matrix)
        new_norms.append(norm_new)
        new_stabs.append(stab_new)
    return (x_local, jnp.stack(new_mats), jnp.stack(new_norms), jnp.stack(new_stabs))


def solution(mesh):
    return jax.shard_map(
        shards,
        mesh=mesh,
        in_specs=(
            P("dp", "tp"),
            P(None, "dp", "tp"),
            P(None, "dp", "tp"),
            P(None, "dp", "tp"),
            P(None, "dp", "tp"),
            P(),
            P(),
            P(None, "dp", "tp"),
            P(),
            P(None, "dp", "tp", None, None),
            P(None, "dp", None, None),
            P(None, "dp", None),
        ),
        out_specs=(
            P("dp", "tp"),
            P(None, "dp", "tp", None, None),
            P(None, "dp", None, None),
            P(None, "dp", None),
        ),
        check_vma=False,
    )
```

profile of v0, /device:TPU:0, one launch (start us, length us, event | category | flops | bytes accessed | tf_op | source)
XLA Modules:
  0.0 442.6 jit_solution(219771178601658571)
XLA Ops:
  7.2 2.8 fusion.75
  10.1 1.3 fusion.76
  11.9 1.3 fusion.77
  13.3 1.3 fusion.78
  15.2 1.3 fusion.74
  19.9 32.4 %all_gather.57 = bf16[8,4096]{1,0:T(8,128)(2,1)S(1)} all-gather(bf16[8,512]{1,0:T(8,128)(2,1)S(1)} %copy-done.11), channel_id=1, replica_groups=mesh['tp'=8,'dp'=4] {'tp'}, dimensions={1}, use_global_device_ids=true | all-gather | bytes 73728 | tf_op jit(solution)/shard_map/all_gather | solution.py:18
  53.9 17.6 %all-gather.23.cloned.1.call-done = bf16[1,4096,384]{2,1,0:T(8,128)(2,1)} async-done(((bf16[1,1024,384]{2,1,0:T(8,128)(2,1)}), bf16[1,4096,384]{2,1,0:T(8,128)(2,1)}) %all-gather.23.cloned.1.call-update) | async-done | bytes 3145744 | tf_op jit(solution)/shard_map/all_gather | solution.py:55
  71.5 30.1 %all-gather.25.cloned.1.call-done = bf16[1,4096,384]{2,1,0:T(8,128)(2,1)} async-done(((bf16[1,1024,384]{2,1,0:T(8,128)(2,1)}), bf16[1,4096,384]{2,1,0:T(8,128)(2,1)}) %all-gather.25.cloned.1.call-update) | async-done | bytes 3145744 | tf_op jit(solution)/shard_map/all_gather | solution.py:56
  101.6 30.0 %all-gather.27.cloned.1.call-done = bf16[1,4096,384]{2,1,0:T(8,128)(2,1)} async-done(((bf16[1,1024,384]{2,1,0:T(8,128)(2,1)}), bf16[1,4096,384]{2,1,0:T(8,128)(2,1)}) %all-gather.27.cloned.1.call-update) | async-done | bytes 3145744 | tf_op jit(solution)/shard_map/all_gather | solution.py:57
  131.6 5.9 %fusion.32 = bf16[8,1536]{1,0:T(8,128)(2,1)S(1)} fusion(bf16[8,4096]{1,0:T(8,128)(2,1)S(1)} %all_gather.57, bf16[4096,384]{1,0:T(8,128)(2,1)} %bitcast.111, bf16[4096,384]{1,0:T(8,128)(2,1)} %bitcast.110, bf16[4096,384]{1,0:T(8,128)(2,1)} %bitcast.109, bf16[4096,384]{1,0:T(8,128)(2,1)} %bitcast.107), kind=kOutput, calls=%fused_computation.33 | convolution fusion | flops 151007232 | bytes 12673024 | tf_op jit(solution)/shard_map/dot_general | solution.py:61
  137.5 30.8 %all_gather.63 = bf16[8,3072]{1,0:T(8,128)(2,1)S(1)} all-gather(bf16[8,384]{1,0:T(8,128)(2,1)S(1)} %get-tuple-element.34), channel_id=1, replica_groups=mesh['tp'=8,'dp'=4] {'tp'}, dimensions={1}, use_global_device_ids=true | all-gather | bytes 55296 | tf_op jit(solution)/shard_map/all_gather | solution.py:68
  168.6 30.8 %all_gather.62 = bf16[8,3072]{1,0:T(8,128)(2,1)S(1)} all-gather(bf16[8,384]{1,0:T(8,128)(2,1)S(1)} %get-tuple-element.35), channel_id=1, replica_groups=mesh['tp'=8,'dp'=4] {'tp'}, dimensions={1}, use_global_device_ids=true | all-gather | bytes 55296 | tf_op jit(solution)/shard_map/all_gather | solution.py:69
  199.5 0.8 reshape.140
  200.6 2.9 fusion.21
  203.5 3.3 fusion.24
  207.0 30.8 %all_gather.64 = bf16[8,3072]{1,0:T(8,128)(2,1)S(1)} all-gather(bf16[8,384]{1,0:T(8,128)(2,1)S(1)} %multiply_convert_fusion.1), channel_id=1, replica_groups=mesh['tp'=8,'dp'=4] {'tp'}, dimensions={1}, use_global_device_ids=true | all-gather | bytes 55296 | tf_op jit(solution)/shard_map/all_gather | solution.py:96
  237.8 2.4 fusion.44
  240.2 30.5 %all_gather.66 = bf16[8,4096]{1,0:T(8,128)(2,1)S(1)} all-gather(bf16[8,512]{1,0:T(8,128)(2,1)S(1)} %fusion.44), channel_id=1, replica_groups=mesh['tp'=8,'dp'=4] {'tp'}, dimensions={1}, use_global_device_ids=true | all-gather | bytes 73728 | tf_op jit(solution)/shard_map/all_gather | solution.py:18
  271.4 11.0 %all-gather.37.cloned.1.call-done = bf16[1,4096,384]{2,1,0:T(8,128)(2,1)} async-done(((bf16[1,1024,384]{2,1,0:T(8,128)(2,1)}), bf16[1,4096,384]{2,1,0:T(8,128)(2,1)}) %all-gather.37.cloned.1.call-update) | async-done | bytes 3145744 | tf_op jit(solution)/shard_map/all_gather | solution.py:57
  282.3 5.9 %fusion.26 = bf16[8,1536]{1,0:T(8,128)(2,1)S(1)} fusion(bf16[8,4096]{1,0:T(8,128)(2,1)S(1)} %fusion.55, bf16[4096,384]{1,0:T(8,128)(2,1)} %bitcast.108, bf16[4096,384]{1,0:T(8,128)(2,1)} %bitcast.106, bf16[4096,384]{1,0:T(8,128)(2,1)} %bitcast.105, bf16[4096,384]{1,0:T(8,128)(2,1)} %bitcast.104), kind=kOutput, calls=%fused_computation.31 | convolution fusion | flops 151007232 | bytes 12673024 | tf_op jit(solution)/shard_map/dot_general | solution.py:61
  288.2 30.8 %all_gather.71 = bf16[8,3072]{1,0:T(8,128)(2,1)S(1)} all-gather(bf16[8,384]{1,0:T(8,128)(2,1)S(1)} %get-tuple-element.32), channel_id=1, replica_groups=mesh['tp'=8,'dp'=4] {'tp'}, dimensions={1}, use_global_device_ids=true | all-gather | bytes 55296 | tf_op jit(solution)/shard_map/all_gather | solution.py:69
  319.1 0.8 reshape.141
  320.0 31.0 %all_gather.72 = bf16[8,3072]{1,0:T(8,128)(2,1)S(1)} all-gather(bf16[8,384]{1,0:T(8,128)(2,1)S(1)} %get-tuple-element.31), channel_id=1, replica_groups=mesh['tp'=8,'dp'=4] {'tp'}, dimensions={1}, use_global_device_ids=true | all-gather | bytes 55296 | tf_op jit(solution)/shard_map/all_gather | solution.py:68
  352.4 2.4 fusion.18
  354.8 3.3 fusion.22
  358.4 32.6 %all_gather.73 = bf16[8,3072]{1,0:T(8,128)(2,1)} all-gather(bf16[8,384]{1,0:T(8,128)(2,1)S(1)} %multiply_convert_fusion), channel_id=1, replica_groups=mesh['tp'=8,'dp'=4] {'tp'}, dimensions={1}, use_global_device_ids=true | all-gather | bytes 55296 | tf_op jit(solution)/shard_map/all_gather | solution.py:96
  390.9 4.5 %multiply_add_fusion.1 = (f32[1,8,24,16,192]{4,3,2,1,0:T(8,128)S(1)}, f32[1,8,24,16,192]{4,3,2,1,0:T(8,128)}) fusion(f32[2,8,24,16,192]{4,3,2,1,0:T(8,128)} %param.21, f32[8,16,192]{2,1,0:T(8,128)S(1)} %get-tuple-element.25, f32[8,24,16]{2,1,0:T(8,128)S(1)} %broadcast_multiply_fusion.3, f32[8,16]{1,0:T(8,128)S(1)} %get-tuple-element.39, ...), kind=kLoop, calls=%fused_computation.30 | loop fusion | flops 3538944 | bytes 9659392 | tf_op jit(solution)/shard_map/add | solution.py:87
  395.5 2.6 fusion.41
  398.0 30.5 %all_gather.75 = bf16[8,4096]{1,0:T(8,128)(2,1)S(1)} all-gather(bf16[8,512]{1,0:T(8,128)(2,1)S(1)} %fusion.41), channel_id=1, replica_groups=mesh['tp'=8,'dp'=4] {'tp'}, dimensions={1}, use_global_device_ids=true | all-gather | bytes 73728 | tf_op jit(solution)/shard_map/all_gather | solution.py:18
  428.9 1.0 multiply_add_fusion.3
  430.0 0.7 pad_maximum_fusion.1
  430.7 3.7 pad_maximum_fusion
  (104 shorter events, 11.0 us)
Async XLA Ops:
  7.2 2.9 copy-start.1
  7.2 46.7 %all-gather.21.cloned.1.call-start = ((), (), s32[]{:S(2)}) async-start(), calls=%async_computation | async-start | bytes 3932160 | tf_op jit(solution)/shard_map/all_gather | solution.py:54
  10.0 1.9 copy-start.2
  10.0 61.5 %all-gather.23.cloned.1.call-start = ((), (), s32[]{:S(2)}) async-start(), calls=%async_computation.1 | async-start | bytes 3932160 | tf_op jit(solution)/shard_map/all_gather | solution.py:55
  11.4 1.9 copy-start.3
  11.4 90.2 %all-gather.25.cloned.1.call-start = ((), (), s32[]{:S(2)}) async-start(), calls=%async_computation.2 | async-start | bytes 3932160 | tf_op jit(solution)/shard_map/all_gather | solution.py:56
  13.2 1.9 copy-start.4
  13.3 118.3 %all-gather.27.cloned.1.call-start = ((), (), s32[]{:S(2)}) async-start(), calls=%async_computation.3 | async-start | bytes 3932160 | tf_op jit(solution)/shard_map/all_gather | solution.py:57
  14.7 223.1 %all-gather.29.cloned.1.call-start = ((), (), s32[]{:S(2)}) async-start(), calls=%async_computation.4 | async-start | bytes 3932160 | tf_op jit(solution)/shard_map/all_gather | solution.py:99
  16.4 3.5 copy-start.11
  16.4 35.8 %copy-start.17 = (f32[2,32]{1,0:T(2,128)S(1)}, f32[2,32]{1,0:T(2,128)}, u32[]{:S(2)}) copy-start(f32[2,32]{1,0:T(2,128)} %param.18) | copy-start | bytes 772
  16.4 35.8 %copy-start.12 = (f32[2,4096]{1,0:T(2,128)S(1)}, f32[2,4096]{1,0:T(2,128)}, u32[]{:S(2)}) copy-start(f32[2,4096]{1,0:T(2,128)} %param.20) | copy-start | bytes 98308
  16.5 35.9 %copy-start.9 = (bf16[2,4096,32]{1,2,0:T(8,128)(2,1)S(1)}, bf16[2,4096,32]{1,2,0:T(8,128)(2,1)}, u32[]{:S(2)}) copy-start(bf16[2,4096,32]{1,2,0:T(8,128)(2,1)} %param.17) | copy-start | bytes 1572868
  16.5 36.0 %copy-start.15 = (f32[2,8,16]{2,1,0:T(8,128)S(1)}, f32[2,8,16]{2,1,0:T(8,128)}, u32[]{:S(2)}) copy-start(f32[2,8,16]{2,1,0:T(8,128)} %param.23) | copy-start | bytes 3076
  16.5 254.8 %all-gather.31.cloned.1.call-start = ((), (), s32[]{:S(2)}) async-start(), calls=%async_computation.5 | async-start | bytes 3932160 | tf_op jit(solution)/shard_map/all_gather | solution.py:54
  17.1 254.3 %all-gather.33.cloned.1.call-start = ((), (), s32[]{:S(2)}) async-start(), calls=%async_computation.6 | async-start | bytes 3932160 | tf_op jit(solution)/shard_map/all_gather | solution.py:55
  17.8 253.5 %all-gather.35.cloned.1.call-start = ((), (), s32[]{:S(2)}) async-start(), calls=%async_computation.7 | async-start | bytes 3932160 | tf_op jit(solution)/shard_map/all_gather | solution.py:56
  18.6 263.8 %all-gather.37.cloned.1.call-start = ((), (), s32[]{:S(2)}) async-start(), calls=%async_computation.8 | async-start | bytes 3932160 | tf_op jit(solution)/shard_map/all_gather | solution.py:57
  19.3 376.1 %all-gather.39.cloned.1.call-start = ((), (), s32[]{:S(2)}) async-start(), calls=%async_computation.9 | async-start | bytes 3932160 | tf_op jit(solution)/shard_map/all_gather | solution.py:99
  131.6 68.9 %copy-start.5 = (f32[2,8,16,192]{3,2,1,0:T(8,128)S(1)}, f32[2,8,16,192]{3,2,1,0:T(8,128)}, u32[]{:S(2)}) copy-start(f32[2,8,16,192]{3,2,1,0:T(8,128)} %param.22) | copy-start | bytes 589828
  271.3 80.1 %copy-start.10 = (bf16[8,4096]{1,0:T(8,128)(2,1)}, bf16[8,4096]{1,0:T(8,128)(2,1)S(1)}, u32[]{:S(2)}) copy-start(bf16[8,4096]{1,0:T(8,128)(2,1)S(1)} %fusion.55) | copy-start | bytes 196612
  352.2 6.1 %copy-start.7 = (f32[8,24,16]{2,1,0:T(8,128)}, f32[8,24,16]{2,1,0:T(8,128)S(1)}, u32[]{:S(2)}) copy-start(f32[8,24,16]{2,1,0:T(8,128)S(1)} %broadcast_multiply_fusion.2) | copy-start | bytes 36868
  395.4 33.5 %copy-start.6 = (f32[2,8,16,192]{3,2,1,0:T(8,128)S(1)}, f32[2,8,16,192]{3,2,1,0:T(8,128)}, u32[]{:S(2)}) copy-start(f32[2,8,16,192]{3,2,1,0:T(8,128)} %param.22) | copy-start | bytes 589828
  395.4 33.5 %copy-start.8 = (f32[1,8,16,192]{3,2,1,0:T(8,128)S(1)}, f32[1,8,16,192]{3,2,1,0:T(8,128)}, u32[]{:S(2)}) copy-start(f32[1,8,16,192]{3,2,1,0:T(8,128)} %reshape.140) | copy-start | bytes 294916
  395.4 35.3 %copy-start = (f32[1,8,24,16,192]{4,3,2,1,0:T(8,128)S(1)}, f32[1,8,24,16,192]{4,3,2,1,0:T(8,128)}, u32[]{:S(2)}) copy-start(f32[1,8,24,16,192]{4,3,2,1,0:T(8,128)} %get-tuple-element.9) | copy-start | bytes 7077892
  430.7 3.7 copy-start.13
  430.7 3.7 copy-start.14
  430.7 4.4 copy-start.16
Sparse Core Ops, SparseCore 0:
  10.1 31.2 all-gather.20
  43.0 28.4 all-gather.22
  73.1 28.4 all-gather.24
  103.0 28.4 all-gather.26
  133.0 28.4 all-gather.28
  162.9 28.4 all-gather.30
  193.0 28.4 all-gather.32
  223.1 28.4 all-gather.34
  253.8 28.4 all-gather.36
  283.8 28.4 all-gather.38
where the time goes:
time: 443 us
  blocking collectives  280 us (63%)
  waiting for transfers between devices  92 us (21%)
  matrix products  23.7 us (5%)
  other arithmetic  19.2 us (4%)
  between operations  14.6 us (3%)
  local copies, waits for them, and re-layouts  12.6 us (3%)
    all_gather x3, blocking collectives, widen_rows(): return lax.all_gather(local_cols, 'tp', axis=1, tiled=True)  93.4 us
    all_gather x2, blocking collectives, shards(): hidden_full = lax.all_gather(hidden, 'tp', axis=1, tiled=True)  63.3 us
    all_gather x2, blocking collectives, shards(): lax.all_gather(query_part, 'tp', axis=1, tiled=True)  61.8 us
    all_gather x2, blocking collectives, shards(): lax.all_gather(key_part, 'tp', axis=1, tiled=True)  61.6 us
    all_gather x2, waiting for transfers between devices, shards(): lax.all_gather(weight_set[3], 'dp', axis=0, tiled=True)  40.9 us
    all_gather x2, waiting for transfers between devices, shards(): lax.all_gather(weight_set[2], 'dp', axis=0, tiled=True)  30.1 us
    all_gather x2, waiting for transfers between devices, shards(): lax.all_gather(weight_set[1], 'dp', axis=0, tiled=True)  17.7 us
    dot_general x2, matrix products, shards(): packed = jnp.dot(columns, joined, preferred_element_type=jnp.float32)  11.8 us
  transfers between devices with their start and end apart: 10, of which 4 were waited for; matrix products, arithmetic and copies ran while one was open for 10% of the time, Pallas kernels for 0%

commit v1 on v0

--- a/solution.py
+++ b/solution.py
@@ -93,7 +93,8 @@
         divisor = jnp.maximum(jnp.abs(denominator), 1.0)
         readout = (numerator / divisor[:, None, :]).reshape(seq_local, col_local)
         hidden = (readout * jax.nn.sigmoid(outgate_part.astype(jnp.float32))).astype(jnp.bfloat16)
-        hidden_full = lax.all_gather(hidden, "tp", axis=1, tiled=True)
+        blocks = lax.all_gather(hidden, "tp")
+        hidden_full = jnp.concatenate(blocks, axis=1)
         branch = jnp.dot(
             hidden_full,
             lax.all_gather(output_weight[block_no], "dp", axis=0, tiled=True),

time: 443 us -> 443 us (level)
  no operation moved by 1% of the time
where the time goes in v1:
time: 443 us
  blocking collectives  280 us (63%)
  waiting for transfers between devices  92 us (21%)
  matrix products  23.7 us (5%)
  other arithmetic  19.2 us (4%)
  between operations  14.6 us (3%)
  local copies, waits for them, and re-layouts  12.6 us (3%)
    all_gather x3, blocking collectives, widen_rows(): return lax.all_gather(local_cols, 'tp', axis=1, tiled=True)  93.4 us
    all_gather x2, blocking collectives, shards(): blocks = lax.all_gather(hidden, 'tp')  63.3 us
    all_gather x2, blocking collectives, shards(): lax.all_gather(query_part, 'tp', axis=1, tiled=True)  61.8 us
    all_gather x2, blocking collectives, shards(): lax.all_gather(key_part, 'tp', axis=1, tiled=True)  61.6 us
    all_gather x2, waiting for transfers between devices, shards(): lax.all_gather(weight_set[3], 'dp', axis=0, tiled=True)  40.9 us
    all_gather x2, waiting for transfers between devices, shards(): lax.all_gather(weight_set[2], 'dp', axis=0, tiled=True)  30.1 us
    all_gather x2, waiting for transfers between devices, shards(): lax.all_gather(weight_set[1], 'dp', axis=0, tiled=True)  17.7 us
    dot_general x2, matrix products, shards(): packed = jnp.dot(columns, joined, preferred_element_type=jnp.float32)  11.8 us
  transfers between devices with their start and end apart: 10, of which 4 were waited for; matrix products, arithmetic and copies ran while one was open for 10% of the time, Pallas kernels for 0%

profile of v1, /device:TPU:0, one launch (start us, length us, event | category | flops | bytes accessed | tf_op | source)
XLA Modules:
  0.0 442.6 jit_solution(15918312324915583625)
XLA Ops:
  7.2 2.8 fusion.75
  10.1 1.3 fusion.76
  11.9 1.3 fusion.77
  13.3 1.3 fusion.78
  15.2 1.3 fusion.74
  19.9 32.4 %all_gather.63 = bf16[8,4096]{1,0:T(8,128)(2,1)S(1)} all-gather(bf16[8,512]{1,0:T(8,128)(2,1)S(1)} %copy-done.11), channel_id=1, replica_groups=mesh['tp'=8,'dp'=4] {'tp'}, dimensions={1}, use_global_device_ids=true | all-gather | bytes 73728 | tf_op jit(solution)/shard_map/all_gather | solution.py:18
  53.9 17.6 %all-gather.25.cloned.1.call-done = bf16[1,4096,384]{2,1,0:T(8,128)(2,1)} async-done(((bf16[1,1024,384]{2,1,0:T(8,128)(2,1)}), bf16[1,4096,384]{2,1,0:T(8,128)(2,1)}) %all-gather.25.cloned.1.call-update) | async-done | bytes 3145744 | tf_op jit(solution)/shard_map/all_gather | solution.py:55
  71.5 30.1 %all-gather.27.cloned.1.call-done = bf16[1,4096,384]{2,1,0:T(8,128)(2,1)} async-done(((bf16[1,1024,384]{2,1,0:T(8,128)(2,1)}), bf16[1,4096,384]{2,1,0:T(8,128)(2,1)}) %all-gather.27.cloned.1.call-update) | async-done | bytes 3145744 | tf_op jit(solution)/shard_map/all_gather | solution.py:56
  101.6 30.0 %all-gather.29.cloned.1.call-done = bf16[1,4096,384]{2,1,0:T(8,128)(2,1)} async-done(((bf16[1,1024,384]{2,1,0:T(8,128)(2,1)}), bf16[1,4096,384]{2,1,0:T(8,128)(2,1)}) %all-gather.29.cloned.1.call-update) | async-done | bytes 3145744 | tf_op jit(solution)/shard_map/all_gather | solution.py:57
  131.6 5.9 %fusion.32 = bf16[8,1536]{1,0:T(8,128)(2,1)S(1)} fusion(bf16[8,4096]{1,0:T(8,128)(2,1)S(1)} %all_gather.63, bf16[4096,384]{1,0:T(8,128)(2,1)} %bitcast.123, bf16[4096,384]{1,0:T(8,128)(2,1)} %bitcast.122, bf16[4096,384]{1,0:T(8,128)(2,1)} %bitcast.121, bf16[4096,384]{1,0:T(8,128)(2,1)} %bitcast.119), kind=kOutput, calls=%fused_computation.33 | convolution fusion | flops 151007232 | bytes 12673024 | tf_op jit(solution)/shard_map/dot_general | solution.py:61
  137.5 30.8 %all_gather.69 = bf16[8,3072]{1,0:T(8,128)(2,1)S(1)} all-gather(bf16[8,384]{1,0:T(8,128)(2,1)S(1)} %get-tuple-element.34), channel_id=1, replica_groups=mesh['tp'=8,'dp'=4] {'tp'}, dimensions={1}, use_global_device_ids=true | all-gather | bytes 55296 | tf_op jit(solution)/shard_map/all_gather | solution.py:68
  168.6 30.8 %all_gather.68 = bf16[8,3072]{1,0:T(8,128)(2,1)S(1)} all-gather(bf16[8,384]{1,0:T(8,128)(2,1)S(1)} %get-tuple-element.35), channel_id=1, replica_groups=mesh['tp'=8,'dp'=4] {'tp'}, dimensions={1}, use_global_device_ids=true | all-gather | bytes 55296 | tf_op jit(solution)/shard_map/all_gather | solution.py:69
  199.5 0.8 reshape.156
  200.6 2.9 fusion.21
  203.5 3.3 fusion.24
  207.0 30.8 %all-gather.4 = bf16[64,384]{1,0:T(8,128)(2,1)S(1)} all-gather(bf16[8,384]{1,0:T(8,128)(2,1)S(1)} %multiply_convert_fusion.1), channel_id=6, replica_groups=mesh['tp'=8,'dp'=4] {'tp'}, dimensions={0}, use_global_device_ids=true | all-gather | bytes 55296 | tf_op jit(solution)/shard_map/all_gather | solution.py:96
  237.8 2.4 fusion.44
  240.2 30.5 %all_gather.73 = bf16[8,4096]{1,0:T(8,128)(2,1)S(1)} all-gather(bf16[8,512]{1,0:T(8,128)(2,1)S(1)} %fusion.44), channel_id=1, replica_groups=mesh['tp'=8,'dp'=4] {'tp'}, dimensions={1}, use_global_device_ids=true | all-gather | bytes 73728 | tf_op jit(solution)/shard_map/all_gather | solution.py:18
  271.4 11.0 %all-gather.39.cloned.1.call-done = bf16[1,4096,384]{2,1,0:T(8,128)(2,1)} async-done(((bf16[1,1024,384]{2,1,0:T(8,128)(2,1)}), bf16[1,4096,384]{2,1,0:T(8,128)(2,1)}) %all-gather.39.cloned.1.call-update) | async-done | bytes 3145744 | tf_op jit(solution)/shard_map/all_gather | solution.py:57
  282.3 5.9 %fusion.26 = bf16[8,1536]{1,0:T(8,128)(2,1)S(1)} fusion(bf16[8,4096]{1,0:T(8,128)(2,1)S(1)} %fusion.55, bf16[4096,384]{1,0:T(8,128)(2,1)} %bitcast.120, bf16[4096,384]{1,0:T(8,128)(2,1)} %bitcast.118, bf16[4096,384]{1,0:T(8,128)(2,1)} %bitcast.117, bf16[4096,384]{1,0:T(8,128)(2,1)} %bitcast.116), kind=kOutput, calls=%fused_computation.31 | convolution fusion | flops 151007232 | bytes 12673024 | tf_op jit(solution)/shard_map/dot_general | solution.py:61
  288.2 30.8 %all_gather.78 = bf16[8,3072]{1,0:T(8,128)(2,1)S(1)} all-gather(bf16[8,384]{1,0:T(8,128)(2,1)S(1)} %get-tuple-element.32), channel_id=1, replica_groups=mesh['tp'=8,'dp'=4] {'tp'}, dimensions={1}, use_global_device_ids=true | all-gather | bytes 55296 | tf_op jit(solution)/shard_map/all_gather | solution.py:69
  319.1 0.8 reshape.157
  320.0 31.0 %all_gather.79 = bf16[8,3072]{1,0:T(8,128)(2,1)S(1)} all-gather(bf16[8,384]{1,0:T(8,128)(2,1)S(1)} %get-tuple-element.31), channel_id=1, replica_groups=mesh['tp'=8,'dp'=4] {'tp'}, dimensions={1}, use_global_device_ids=true | all-gather | bytes 55296 | tf_op jit(solution)/shard_map/all_gather | solution.py:68
  352.4 2.4 fusion.18
  354.8 3.3 fusion.22
  358.4 32.6 %all-gather.10 = bf16[64,384]{1,0:T(8,128)(2,1)} all-gather(bf16[8,384]{1,0:T(8,128)(2,1)S(1)} %multiply_convert_fusion), channel_id=12, replica_groups=mesh['tp'=8,'dp'=4] {'tp'}, dimensions={0}, use_global_device_ids=true | all-gather | bytes 55296 | tf_op jit(solution)/shard_map/all_gather | solution.py:96
  390.9 4.5 %multiply_add_fusion.1 = (f32[1,8,24,16,192]{4,3,2,1,0:T(8,128)S(1)}, f32[1,8,24,16,192]{4,3,2,1,0:T(8,128)}) fusion(f32[2,8,24,16,192]{4,3,2,1,0:T(8,128)} %param.21, f32[8,16,192]{2,1,0:T(8,128)S(1)} %get-tuple-element.25, f32[8,24,16]{2,1,0:T(8,128)S(1)} %broadcast_multiply_fusion.3, f32[8,16]{1,0:T(8,128)S(1)} %get-tuple-element.39, ...), kind=kLoop, calls=%fused_computation.30 | loop fusion | flops 3538944 | bytes 9659392 | tf_op jit(solution)/shard_map/add | solution.py:87
  395.5 2.6 fusion.41
  398.0 30.5 %all_gather.83 = bf16[8,4096]{1,0:T(8,128)(2,1)S(1)} all-gather(bf16[8,512]{1,0:T(8,128)(2,1)S(1)} %fusion.41), channel_id=1, replica_groups=mesh['tp'=8,'dp'=4] {'tp'}, dimensions={1}, use_global_device_ids=true | all-gather | bytes 73728 | tf_op jit(solution)/shard_map/all_gather | solution.py:18
  428.9 1.0 multiply_add_fusion.3
  430.0 0.7 pad_maximum_fusion.1
  430.7 3.7 pad_maximum_fusion
  (104 shorter events, 11.0 us)
Async XLA Ops:
  7.2 2.9 copy-start.1
  7.2 46.7 %all-gather.23.cloned.1.call-start = ((), (), s32[]{:S(2)}) async-start(), calls=%async_computation | async-start | bytes 3932160 | tf_op jit(solution)/shard_map/all_gather | solution.py:54
  10.0 1.9 copy-start.2
  10.0 61.5 %all-gather.25.cloned.1.call-start = ((), (), s32[]{:S(2)}) async-start(), calls=%async_computation.1 | async-start | bytes 3932160 | tf_op jit(solution)/shard_map/all_gather | solution.py:55
  11.4 1.9 copy-start.3
  11.4 90.2 %all-gather.27.cloned.1.call-start = ((), (), s32[]{:S(2)}) async-start(), calls=%async_computation.2 | async-start | bytes 3932160 | tf_op jit(solution)/shard_map/all_gather | solution.py:56
  13.2 1.9 copy-start.4
  13.3 118.3 %all-gather.29.cloned.1.call-start = ((), (), s32[]{:S(2)}) async-start(), calls=%async_computation.3 | async-start | bytes 3932160 | tf_op jit(solution)/shard_map/all_gather | solution.py:57
  14.7 223.1 %all-gather.31.cloned.1.call-start = ((), (), s32[]{:S(2)}) async-start(), calls=%async_computation.4 | async-start | bytes 3932160 | tf_op jit(solution)/shard_map/all_gather | solution.py:100
  16.4 3.5 copy-start.11
  16.4 35.8 %copy-start.17 = (f32[2,32]{1,0:T(2,128)S(1)}, f32[2,32]{1,0:T(2,128)}, u32[]{:S(2)}) copy-start(f32[2,32]{1,0:T(2,128)} %param.18) | copy-start | bytes 772
  16.4 35.8 %copy-start.12 = (f32[2,4096]{1,0:T(2,128)S(1)}, f32[2,4096]{1,0:T(2,128)}, u32[]{:S(2)}) copy-start(f32[2,4096]{1,0:T(2,128)} %param.20) | copy-start | bytes 98308
  16.5 35.9 %copy-start.9 = (bf16[2,4096,32]{1,2,0:T(8,128)(2,1)S(1)}, bf16[2,4096,32]{1,2,0:T(8,128)(2,1)}, u32[]{:S(2)}) copy-start(bf16[2,4096,32]{1,2,0:T(8,128)(2,1)} %param.17) | copy-start | bytes 1572868
  16.5 36.0 %copy-start.15 = (f32[2,8,16]{2,1,0:T(8,128)S(1)}, f32[2,8,16]{2,1,0:T(8,128)}, u32[]{:S(2)}) copy-start(f32[2,8,16]{2,1,0:T(8,128)} %param.23) | copy-start | bytes 3076
  16.5 254.8 %all-gather.33.cloned.1.call-start = ((), (), s32[]{:S(2)}) async-start(), calls=%async_computation.5 | async-start | bytes 3932160 | tf_op jit(solution)/shard_map/all_gather | solution.py:54
  17.1 254.3 %all-gather.35.cloned.1.call-start = ((), (), s32[]{:S(2)}) async-start(), calls=%async_computation.6 | async-start | bytes 3932160 | tf_op jit(solution)/shard_map/all_gather | solution.py:55
  17.8 253.5 %all-gather.37.cloned.1.call-start = ((), (), s32[]{:S(2)}) async-start(), calls=%async_computation.7 | async-start | bytes 3932160 | tf_op jit(solution)/shard_map/all_gather | solution.py:56
  18.6 263.8 %all-gather.39.cloned.1.call-start = ((), (), s32[]{:S(2)}) async-start(), calls=%async_computation.8 | async-start | bytes 3932160 | tf_op jit(solution)/shard_map/all_gather | solution.py:57
  19.3 376.1 %all-gather.41.cloned.1.call-start = ((), (), s32[]{:S(2)}) async-start(), calls=%async_computation.9 | async-start | bytes 3932160 | tf_op jit(solution)/shard_map/all_gather | solution.py:100
  131.6 68.9 %copy-start.5 = (f32[2,8,16,192]{3,2,1,0:T(8,128)S(1)}, f32[2,8,16,192]{3,2,1,0:T(8,128)}, u32[]{:S(2)}) copy-start(f32[2,8,16,192]{3,2,1,0:T(8,128)} %param.22) | copy-start | bytes 589828
  271.3 80.1 %copy-start.10 = (bf16[8,4096]{1,0:T(8,128)(2,1)}, bf16[8,4096]{1,0:T(8,128)(2,1)S(1)}, u32[]{:S(2)}) copy-start(bf16[8,4096]{1,0:T(8,128)(2,1)S(1)} %fusion.55) | copy-start | bytes 196612
  352.2 6.1 %copy-start.7 = (f32[8,24,16]{2,1,0:T(8,128)}, f32[8,24,16]{2,1,0:T(8,128)S(1)}, u32[]{:S(2)}) copy-start(f32[8,24,16]{2,1,0:T(8,128)S(1)} %broadcast_multiply_fusion.2) | copy-start | bytes 36868
  395.4 33.5 %copy-start.6 = (f32[2,8,16,192]{3,2,1,0:T(8,128)S(1)}, f32[2,8,16,192]{3,2,1,0:T(8,128)}, u32[]{:S(2)}) copy-start(f32[2,8,16,192]{3,2,1,0:T(8,128)} %param.22) | copy-start | bytes 589828
  395.4 33.5 %copy-start.8 = (f32[1,8,16,192]{3,2,1,0:T(8,128)S(1)}, f32[1,8,16,192]{3,2,1,0:T(8,128)}, u32[]{:S(2)}) copy-start(f32[1,8,16,192]{3,2,1,0:T(8,128)} %reshape.156) | copy-start | bytes 294916
  395.4 35.3 %copy-start = (f32[1,8,24,16,192]{4,3,2,1,0:T(8,128)S(1)}, f32[1,8,24,16,192]{4,3,2,1,0:T(8,128)}, u32[]{:S(2)}) copy-start(f32[1,8,24,16,192]{4,3,2,1,0:T(8,128)} %get-tuple-element.9) | copy-start | bytes 7077892
  430.7 3.7 copy-start.13
  430.7 3.7 copy-start.14
  430.7 4.4 copy-start.16
Sparse Core Ops, SparseCore 0:
  10.1 31.2 all-gather.22
  43.0 28.4 all-gather.24
  73.1 28.4 all-gather.26
  103.0 28.4 all-gather.28
  133.0 28.4 all-gather.30
  162.9 28.4 all-gather.32
  193.0 28.4 all-gather.34
  223.1 28.4 all-gather.36
  253.8 28.4 all-gather.38
  283.8 28.4 all-gather.40
